TPU v7x, 32 devices: a whole 2x2x4 slice. The times are simulated.
32 devices in a mesh: ep: 8 (over z, core), tp: 4 (over y, x).
Axes of the slice: x: 2, y: 2, z: 4, core: 2. Of those that a mesh axis runs over, the one named last changes fastest.
Arguments:
- query_proj: bfloat16 [4096, 1024], P('ep', 'tp'), may hold values from -6 to 6
- key_proj: bfloat16 [4096, 256], P('ep'), may hold values from -6 to 6
- value_proj: bfloat16 [4096, 256], P('ep'), may hold values from -24 to 24
- sink_logit: float32 [16], P('tp'), may hold values from 2 to 6
- out_weight: bfloat16 [1024, 2048], P(None, 'tp'), may hold values from -0.1875 to 0.1875
- expert_input: bfloat16 [2048, 2048], P('ep'), may hold values from -6 to 6
- norm_gain: float32 [2048], replicated, may hold values from 0.1 to 1.9
- routes: int32 [2048, 2], P('ep'), may hold values from 0 to 7, as said below
- route_weights: float32 [2048, 2], P('ep'), may hold values from 0.2 to 1
- gate_weight: bfloat16 [8, 2048, 4096], P('ep', None, 'tp'), may hold values from -0.125 to 0.125
- up_weight: bfloat16 [8, 2048, 4096], P('ep', None, 'tp'), may hold values from -0.125 to 0.125
- down_weight: bfloat16 [8, 4096, 2048], P('ep', 'tp'), may hold values from -0.09375 to 0.09375
Outputs:
- mixer_out: bfloat16 [4096, 2048], P('ep', 'tp')
- expert_out: bfloat16 [2048, 2048], P('ep', 'tp')
Inputs may be any that keep to these rules, and one draw needn't show every extreme that they name: `routes`: experts form 4 groups of consecutive numbers of equal size. Each row names 2 different experts of one group. In each aligned block of 256 rows no expert is named by more than 128 rows, and in every block some expert is named by exactly 128 rows.
All inputs are finite; a program needn't handle non-finite values.
Results may differ from a plain program's by a relative error of at most 0.017.
Values may be sent and summed in bfloat16 or wider, within the bound.
A program may use at most 64 MiB of HBM per device.

v0:
```python
import jax
import jax.numpy as jnp
import numpy as np
from jax import lax
from jax.experimental import pallas as pl
from jax.experimental.pallas import tpu as pltpu
from jax.sharding import PartitionSpec as P

D = 2048
HEADS = 16
KV_HEADS = 4
HEAD_DIM = 64
HALF_WIN = 128
GROUPS = 4
TOP_K = 2


NORM_EPS = 1e-06
ROPE_BASE = 10000.0
NEG_BIG = -1e30
MESH = pl.DeviceIdType.MESH
SIDE = 128


def padded(block, sides, width):
    for axis, dim in sides:
        count = lax.axis_size(axis)
        forward = [(i, i + 1) for i in range(count - 1)]
        backward = [(target, source) for source, target in forward]
        low = lax.ppermute(
            lax.slice_in_dim(block, block.shape[dim] - width, None, axis=dim), axis, forward
        )
        high = lax.ppermute(lax.slice_in_dim(block, 0, width, axis=dim), axis, backward)
        block = jnp.concatenate([low, block, high], axis=dim)
    return block


def rotate(features, position_start):
    count = features.shape[0]
    half_dim = features.shape[-1] // 2
    inverse_freq = 1.0 / ROPE_BASE ** (
        jnp.arange(half_dim, dtype=jnp.float32) * 2.0 / features.shape[-1]
    )
    position = (jnp.arange(count, dtype=jnp.int32) + position_start).astype(jnp.float32)
    angles = position[:, None] * inverse_freq[None, :]
    cosine = jnp.cos(angles)[:, None, :]
    sine_part = jnp.sin(angles)[:, None, :]
    lower_half = features[..., :half_dim]
    upper_half = features[..., half_dim:]
    return jnp.concatenate(
        [
            lower_half * cosine - upper_half * sine_part,
            upper_half * cosine + lower_half * sine_part,
        ],
        axis=-1,
    )


def mixer_half(query_proj, key_proj, value_proj, sink_logit, out_weight):
    row_count = query_proj.shape[0]
    local_heads = query_proj.shape[1] // HEAD_DIM
    per_kv = HEADS // KV_HEADS
    kv_local = max(1, local_heads // per_kv)
    group_size = local_heads // kv_local
    tp_index = lax.axis_index("tp")
    offset = lax.axis_index("ep") * row_count
    seq_total = row_count * lax.axis_size("ep")
    first_kv = tp_index * local_heads // per_kv
    own_keys = lax.dynamic_slice_in_dim(key_proj, first_kv * HEAD_DIM, kv_local * HEAD_DIM, 1)
    own_values = lax.dynamic_slice_in_dim(value_proj, first_kv * HEAD_DIM, kv_local * HEAD_DIM, 1)
    rot_q = rotate(
        query_proj.reshape(row_count, local_heads, HEAD_DIM).astype(jnp.float32), offset
    ).astype(jnp.bfloat16)
    rot_k = rotate(
        own_keys.reshape(row_count, kv_local, HEAD_DIM).astype(jnp.float32), offset
    ).astype(jnp.bfloat16)
    stacked = jnp.stack([rot_k, own_values.reshape(row_count, kv_local, HEAD_DIM)])
    extended = padded(stacked, (("ep", 1),), HALF_WIN)
    own_sink = sink_logit.reshape(kv_local, group_size)
    block_rows = min(512, row_count)
    key_rows = block_rows + 2 * HALF_WIN
    key_offset = jnp.arange(key_rows, dtype=jnp.int32) - HALF_WIN
    key_gap = key_offset[None, :] - jnp.arange(block_rows, dtype=jnp.int32)[:, None]
    query_block = rot_q.reshape(block_rows, kv_local, group_size, HEAD_DIM)
    key_block = extended[0, 0:key_rows]
    value_block = extended[1, 0:key_rows]
    scores = jnp.einsum(
        "qngd,knd->ngqk", query_block, key_block, preferred_element_type=jnp.float32
    ) * HEAD_DIM ** (-0.5)
    global_key = offset + 0 + key_offset
    allowed = (
        (jnp.abs(key_gap) <= HALF_WIN)
        & (global_key >= 0)[None, :]
        & (global_key < seq_total)[None, :]
    )
    scores = jnp.where(allowed[None, None], scores, NEG_BIG)
    row_peak = jnp.maximum(jnp.max(scores, axis=-1), own_sink[:, :, None])
    lifted = jnp.exp(scores - row_peak[..., None])
    norm_total = jnp.sum(lifted, axis=-1) + jnp.exp(own_sink[:, :, None] - row_peak)
    probs = (lifted / norm_total[..., None]).astype(jnp.bfloat16)
    weighted = jnp.einsum("ngqk,knd->qngd", probs, value_block, preferred_element_type=jnp.float32)
    pieces = weighted.astype(jnp.bfloat16).reshape(block_rows, local_heads * HEAD_DIM)
    projected = jnp.dot(
        lax.all_gather(pieces, "tp", axis=1, tiled=True),
        out_weight,
        preferred_element_type=jnp.float32,
    )
    return projected.astype(jnp.bfloat16)


def expert_half(
    expert_input, norm_gain, routes, route_weights, gate_weight, up_weight, down_weight
):
    row_count = expert_input.shape[0]
    widened = expert_input.astype(jnp.float32)
    normed = (
        widened
        * lax.rsqrt(jnp.mean(widened * widened, axis=1, keepdims=True) + NORM_EPS)
        * norm_gain
    ).astype(jnp.bfloat16)
    local_experts = gate_weight.shape[0]
    ep_count = lax.axis_size("ep")
    expert_count = local_experts * ep_count
    capacity = row_count * GROUPS // expert_count
    col_count = D // lax.axis_size("tp")
    flat_routes = routes.reshape(-1)
    onehot = (flat_routes[:, None] == jnp.arange(expert_count, dtype=jnp.int32)[None, :]).astype(
        jnp.int32
    )
    slot_rank = jnp.sum((jnp.cumsum(onehot, axis=0) - onehot) * onehot, axis=1)
    slot_index = flat_routes * capacity + slot_rank
    source_rows = jnp.arange(row_count * TOP_K, dtype=jnp.int32) // TOP_K
    own_cols = lax.dynamic_slice_in_dim(normed, lax.axis_index("tp") * col_count, col_count, 1)
    outgoing = (
        jnp.zeros((expert_count * capacity, col_count), jnp.bfloat16)
        .at[slot_index]
        .set(own_cols[source_rows])
    )
    arrived = lax.all_to_all(
        outgoing.reshape(expert_count, capacity, col_count),
        "ep",
        split_axis=0,
        concat_axis=1,
        tiled=True,
    )
    shard_piece = lax.all_gather(arrived, "tp", axis=2, tiled=True)
    gate_sum = jnp.einsum(
        "esd,edh->esh", shard_piece, gate_weight, preferred_element_type=jnp.float32
    )
    up_sum = jnp.einsum("esd,edh->esh", shard_piece, up_weight, preferred_element_type=jnp.float32)
    hidden = (jax.nn.silu(gate_sum) * up_sum).astype(jnp.bfloat16)
    slot_total = hidden.shape[1]
    term = jnp.einsum("esh,ehc->ces", hidden, down_weight, preferred_element_type=jnp.float32)
    summed = lax.psum_scatter(
        term.reshape(col_count * lax.axis_size("tp"), local_experts * slot_total).astype(
            jnp.bfloat16
        ),
        "tp",
        scatter_dimension=0,
        tiled=True,
    )
    result = summed.reshape(col_count, local_experts, ep_count, capacity)
    returned = lax.all_to_all(result, "ep", split_axis=2, concat_axis=1, tiled=True)
    returned = returned.reshape(col_count, expert_count * capacity)
    picked = (
        jnp.take(returned, slot_index, axis=1)
        .reshape(col_count, row_count, TOP_K)
        .astype(jnp.float32)
    )
    combined = jnp.sum(picked * route_weights[None, :, :], axis=2)
    return combined.T.astype(jnp.bfloat16)


def local(
    query_proj,
    key_proj,
    value_proj,
    sink_logit,
    out_weight,
    expert_input,
    norm_gain,
    routes,
    route_weights,
    gate_weight,
    up_weight,
    down_weight,
):
    mixer_out = mixer_half(query_proj, key_proj, value_proj, sink_logit, out_weight)
    expert_out = expert_half(
        expert_input, norm_gain, routes, route_weights, gate_weight, up_weight, down_weight
    )
    return (mixer_out, expert_out)


def fits_fused(mesh):
    return (
        mesh.shape["tp"] == 4
        and mesh.shape["ep"] == 2 * GROUPS
        and HALF_WIN == SIDE
        and HEADS // KV_HEADS == 4
        and KV_HEADS == 4
    )


class Slots:
    def __init__(self):
        self.names = {}

    def __call__(self, *name):
        return self.names.setdefault(name, len(self.names))


COPY_SLOTS = 96


def fused_kernel(
    q_ref, key_ref, value_ref, cos_far, sin_far, cos_near, sin_near, sink_ref,
    x_ref, gain_ref, routes_ref, rw_ref,
    wout_hbm, wg_hbm, wu_hbm, wd_hbm,
    mixer_ref, expert_ref,
    wout, wg, wu, wd, kve, krot, att, sel_ret, snd, xs, hid, yb, yr, zs, rx, ry, sb, r2, fin, ret,
    ssem, rsem, wsem,
):
    ep = lax.axis_index("ep")
    t = lax.axis_index("tp")
    chips = GROUPS
    z, core = ep // 2, ep % 2
    partner = ep + 1 - 2 * core
    other = (ep + 2 * core - 1 + 2 * chips) % (2 * chips)
    up, down = (ep + 1) % (2 * chips), (ep + 2 * chips - 1) % (2 * chips)
    ty, tx = t // 2, t % 2
    t_x, t_y, t_d = ty * 2 + 1 - tx, (1 - ty) * 2 + tx, (1 - ty) * 2 + 1 - tx
    rows = q_ref.shape[0]
    tokens, model = x_ref.shape
    cap = xs.shape[1] // 2
    part = cap // 4
    half_part, half_cap = part // 2, cap // 2
    hidden = wg.shape[1]
    cols = wout.shape[1]
    slots = Slots()
    started = []

    def send(name, src, dst, device):
        index = slots(*name)
        copy = pltpu.make_async_remote_copy(
            src_ref=src, dst_ref=dst, send_sem=ssem.at[index], recv_sem=rsem.at[index],
            device_id=device, device_id_type=MESH,
        )
        copy.start()
        started.append(copy)

    def arrive(name, dst):
        index = slots(*name)
        pltpu.make_async_remote_copy(
            src_ref=dst, dst_ref=dst, send_sem=ssem.at[index], recv_sem=rsem.at[index],
            device_id=(ep, t_x), device_id_type=MESH,
        ).wait_recv()

    def loads():
        pairs = ((wg_hbm, wg), (wu_hbm, wu), (wd_hbm, wd), (wout_hbm, wout))
        return [pltpu.make_async_copy(a, b, wsem.at[i]) for i, (a, b) in enumerate(pairs)]

    weight_loads = loads()
    for copy in weight_loads:
        copy.start()

    barrier = pltpu.get_barrier_semaphore()
    peers = [((z + k) % chips * 2 + core, t) for k in range(1, chips)]
    peers += [(ep, t_x), (ep, t_y), (partner, t), (other, t)]
    for peer in peers:
        pl.semaphore_signal(barrier, inc=1, device_id=peer, device_id_type=MESH)

    row_i = lax.broadcasted_iota(jnp.int32, (key_ref.shape[1], 2 * HEAD_DIM), 0)
    col_i = lax.broadcasted_iota(jnp.int32, (key_ref.shape[1], 2 * HEAD_DIM), 1)
    own_key = jnp.where((row_i == t * HEAD_DIM + col_i) & (col_i < HEAD_DIM), 1.0, 0.0)
    own_value = jnp.where(
        (row_i == (t - 1) * HEAD_DIM + col_i) & (col_i >= HEAD_DIM), 1.0, 0.0
    )
    both = jnp.dot(
        key_ref[...], own_key.astype(jnp.bfloat16), preferred_element_type=jnp.float32
    ) + jnp.dot(
        value_ref[...], own_value.astype(jnp.bfloat16), preferred_element_type=jnp.float32
    )
    kve[SIDE : SIDE + rows, :] = both.astype(jnp.bfloat16)
    wide = x_ref[...].astype(jnp.float32)
    inverse = lax.rsqrt(jnp.mean(wide * wide, axis=1, keepdims=True) + NORM_EPS)
    normed = (wide * inverse * gain_ref[...]).astype(jnp.bfloat16)
    group = routes_ref[0:1, :] >> 1
    row_i = lax.broadcasted_iota(jnp.int32, (tokens, tokens), 0)
    col_i = lax.broadcasted_iota(jnp.int32, (tokens, tokens), 1)
    later = jnp.where(row_i < col_i, 1.0, 0.0).astype(jnp.bfloat16)
    hot = jnp.where(lax.broadcasted_iota(jnp.int32, (16, tokens), 0) == group, 1.0, 0.0)
    count = jnp.dot(hot.astype(jnp.bfloat16), later, preferred_element_type=jnp.float32)
    rank = jnp.sum(count * hot, axis=0, keepdims=True).astype(jnp.int32)

    slot = lax.broadcasted_iota(jnp.int32, (chips * part, tokens), 0)
    slot_group = lax.rem(z - slot // part + chips, chips)
    pick = (group == slot_group) & (rank == t * part + lax.rem(slot, part))
    pick = jnp.where(pick, 1.0, 0.0).astype(jnp.bfloat16)

    def select_back():
        slot = lax.broadcasted_iota(jnp.int32, (chips * cap, tokens), 0)
        slot_group = lax.rem(z - slot // cap + chips, chips)
        place = (group == slot_group) & (rank == lax.rem(slot, cap))
        sel_ret[...] = jnp.where(place, 1.0, 0.0).T.astype(jnp.bfloat16)

    odd = (routes_ref[...] & 1) == 1
    weight_odd = jnp.sum(jnp.where(odd, rw_ref[...], 0.0), axis=0, keepdims=True)
    weight_even = jnp.sum(jnp.where(odd, 0.0, rw_ref[...]), axis=0, keepdims=True)
    lane = lax.broadcasted_iota(jnp.int32, (128, tokens), 0)
    weight = jnp.where(lane < 2, weight_even, weight_odd)
    high = weight.astype(jnp.bfloat16).astype(jnp.float32)
    weight = jnp.where((lane & 1) == 0, high, weight - high)
    weight = jnp.where(lane < 4, weight, 0.0).astype(jnp.bfloat16)
    snd[:, model:] = lax.dot_general(
        pick, weight, (((1,), (1,)), ((), ())), preferred_element_type=jnp.float32
    ).astype(jnp.bfloat16)
    snd[:, :model] = jnp.dot(pick, normed, preferred_element_type=jnp.float32).astype(jnp.bfloat16)

    def piece(k, owner_t, start=0, count=part):
        first = pl.multiple_of(core * cap + owner_t * part + start, 16)
        return xs.at[k, pl.ds(first, count)]

    xs[0, pl.ds(pl.multiple_of(core * cap + t * part, 16), part), :] = snd[0:part, :]

    pl.semaphore_wait(barrier, len(peers))
    send(("halo", 0), kve.at[pl.ds(rows, SIDE)], kve.at[pl.ds(0, SIDE)], (up, t))
    send(("halo", 1), kve.at[pl.ds(SIDE, SIDE)], kve.at[pl.ds(SIDE + rows, SIDE)], (down, t))
    for k in (1, 2, 3):
        send(
            ("z", k), snd.at[pl.ds(k * part, part)], piece(k, t),
            ((z - k + chips) % chips * 2 + core, t),
        )

    def spread(k):
        if k:
            arrive(("z", k), piece(k, t))
        send(("x", k), piece(k, t), piece(k, t), (ep, t_x))
        send(("y", k), piece(k, t), piece(k, t), (ep, t_y))

    def relay(k):
        arrive(("x", k), piece(k, t_x))
        send(
            ("da", k), piece(k, t_x, 0, half_part), piece(k, t_x, 0, half_part), (ep, t_y)
        )
        arrive(("y", k), piece(k, t_y))
        send(
            ("db", k), piece(k, t_y, half_part, half_part),
            piece(k, t_y, half_part, half_part), (ep, t_x),
        )

    def own_rows(k, which):
        return xs.at[k, pl.ds(pl.multiple_of(which * cap, 16), cap)]

    def share(k):
        arrive(("da", k), piece(k, t_d, 0, half_part))
        arrive(("db", k), piece(k, t_d, half_part, half_part))
        send(("p", k), own_rows(k, core), own_rows(k, core), (partner, t))

    def swap_matrix(size):
        i = lax.broadcasted_iota(jnp.int32, (size, size), 0)
        j = lax.broadcasted_iota(jnp.int32, (size, size), 1)
        half = HEAD_DIM // 2
        low = (j & (HEAD_DIM - 1)) < half
        minus = low & (i == j + half)
        plus = (~low) & (i == j - half)
        return jnp.where(minus, -1.0, jnp.where(plus, 1.0, 0.0)).astype(jnp.bfloat16)

    def tables(block):
        far_c, far_s = cos_far[block : block + 1, :], sin_far[block : block + 1, :]
        near_c, near_s = cos_near[...], sin_near[...]
        return far_c * near_c - far_s * near_s, far_s * near_c + far_c * near_s

    def rotate_keys():
        swap = swap_matrix(2 * HEAD_DIM)
        for block in range(rows // SIDE + 2):
            cosine, sine = tables(block)
            raw = kve[block * SIDE : (block + 1) * SIDE, :]
            turned = jnp.dot(raw, swap, preferred_element_type=jnp.float32)
            krot[block * SIDE : (block + 1) * SIDE, :] = (
                raw.astype(jnp.float32) * cosine + turned * sine
            ).astype(jnp.bfloat16)

    heads = HEADS // KV_HEADS

    def attend(block):
        swap = swap_matrix(heads * HEAD_DIM)
        cosine, sine = tables(block + 1)
        cosine = jnp.concatenate([cosine] * (heads // 2), axis=1)
        sine = jnp.concatenate([sine] * (heads // 2), axis=1)
        raw = q_ref[block * SIDE : (block + 1) * SIDE, :]
        turned = jnp.dot(raw, swap, preferred_element_type=jnp.float32)
        query = (
            (raw.astype(jnp.float32) * cosine + turned * sine) * HEAD_DIM ** (-0.5)
        ).astype(jnp.bfloat16)
        query = jnp.concatenate(
            [query[:, h * HEAD_DIM : (h + 1) * HEAD_DIM] for h in range(heads)], axis=0
        )
        span = 3 * SIDE
        keys = krot[block * SIDE : block * SIDE + span, :HEAD_DIM]
        values = kve[block * SIDE : block * SIDE + span, HEAD_DIM:]
        scores = lax.dot_general(
            query, keys, (((1,), (1,)), ((), ())), preferred_element_type=jnp.float32
        )
        row = lax.broadcasted_iota(jnp.int32, scores.shape, 0) & (SIDE - 1)
        col = lax.broadcasted_iota(jnp.int32, scores.shape, 1)
        gap = col - row
        absolute = col + (ep * rows + (block - 1) * SIDE)
        allowed = (gap >= 0) & (gap <= 2 * HALF_WIN)
        allowed = allowed & (absolute >= 0) & (absolute < rows * 2 * chips)
        scores = jnp.where(allowed, scores, NEG_BIG)
        head = lax.broadcasted_iota(jnp.int32, (heads * SIDE, 1), 0) // SIDE
        sink = jnp.zeros((heads * SIDE, 1), jnp.float32)
        for h in range(heads):
            sink = jnp.where(head == h, sink_ref[h], sink)
        peak = jnp.maximum(jnp.max(scores, axis=1, keepdims=True), sink)
        lifted = jnp.exp(scores - peak)
        total = jnp.sum(lifted, axis=1, keepdims=True) + jnp.exp(sink - peak)
        out = jnp.dot(lifted.astype(jnp.bfloat16), values, preferred_element_type=jnp.float32)
        out = (out / total).astype(jnp.bfloat16)
        att[t, block * SIDE : (block + 1) * SIDE, :] = jnp.concatenate(
            [out[h * SIDE : (h + 1) * SIDE, :] for h in range(heads)], axis=1
        )

    def widen(k, half):
        if half == 0:
            arrive(("p", k), own_rows(k, 1 - core))
        tag = xs[k, :, model:].astype(jnp.float32)
        lane = lax.broadcasted_iota(jnp.int32, tag.shape, 1)
        weight = jnp.sum(jnp.where(lane // 2 == core, tag, 0.0), axis=1, keepdims=True)
        tile = 256
        count = hidden // tile // 2

        @pl.loop(half * count, (half + 1) * count)
        def _(i):
            at = pl.ds(pl.multiple_of(i * tile, tile), tile)
            gate = jnp.dot(xs[k, :, :model], wg[:, at], preferred_element_type=jnp.float32)
            lift = jnp.dot(xs[k, :, :model], wu[:, at], preferred_element_type=jnp.float32)
            value = gate / (1.0 + jnp.exp(-gate)) * lift
            hid[:, at] = (value * weight).astype(jnp.bfloat16)

    def narrow(k):
        @pl.loop(0, model // cols)
        def _(i):
            at = pl.ds(pl.multiple_of(i * cols, cols), cols)
            yb[k, i] = jnp.dot(
                hid[...], wd[:, at], preferred_element_type=jnp.float32
            ).astype(jnp.bfloat16)

        theirs = pl.ds(pl.multiple_of((1 - core) * cap, 16), cap)
        send(("q", k), yb.at[k, :, theirs], yr.at[k], (partner, t))

    def add(*parts):
        return sum(p.astype(jnp.float32) for p in parts).astype(jnp.bfloat16)

    first, second = slice(0, half_cap), slice(half_cap, cap)
    d_first, d_second = pl.ds(0, half_cap), pl.ds(half_cap, half_cap)

    def scatter_one(k):
        arrive(("q", k), yr.at[k])
        mine = pl.ds(pl.multiple_of(core * cap, 16), cap)
        zs[k] = add(yb[k, :, mine], yr[k])
        send(("rx", k, 1), zs.at[k, t_d, d_first], rx.at[k, 1], (ep, t_x))
        send(("ry", k, 1), zs.at[k, t_d, d_second], ry.at[k, 1], (ep, t_y))
        send(("rx", k, 0), zs.at[k, t_x, d_first], rx.at[k, 0], (ep, t_x))
        send(("ry", k, 0), zs.at[k, t_y, d_second], ry.at[k, 0], (ep, t_y))

    def scatter_two(k):
        arrive(("rx", k, 1), rx.at[k, 1])
        sb[k, 0] = add(zs[k, t_y, first], rx[k, 1])
        send(("r2", k, 0), sb.at[k, 0], r2.at[k, 0], (ep, t_y))
        arrive(("ry", k, 1), ry.at[k, 1])
        sb[k, 1] = add(zs[k, t_x, second], ry[k, 1])
        send(("r2", k, 1), sb.at[k, 1], r2.at[k, 1], (ep, t_x))

    def give_back(k):
        arrive(("rx", k, 0), rx.at[k, 0])
        arrive(("ry", k, 0), ry.at[k, 0])
        arrive(("r2", k, 0), r2.at[k, 0])
        arrive(("r2", k, 1), r2.at[k, 1])
        target = fin if k else ret
        target[k, first] = add(zs[k, t, first], rx[k, 0], r2[k, 0])
        target[k, second] = add(zs[k, t, second], ry[k, 0], r2[k, 1])
        if k:
            send(("ret", k), fin.at[k], ret.at[k], ((z + k) % chips * 2 + core, t))

    def wait_back(k):
        arrive(("ret", k), ret.at[k])

    half_rows = rows // 2

    def attended_out():
        send(("ax",), att.at[t], att.at[t], (ep, t_x))
        send(("ay",), att.at[t], att.at[t], (ep, t_y))

    def attended_relay():
        low, high = pl.ds(0, half_rows), pl.ds(half_rows, half_rows)
        arrive(("ax",), att.at[t_x])
        send(("ada",), att.at[t_x, low], att.at[t_x, low], (ep, t_y))
        arrive(("ay",), att.at[t_y])
        send(("adb",), att.at[t_y, high], att.at[t_y, high], (ep, t_x))

    def project():
        arrive(("ada",), att.at[t_d, pl.ds(0, half_rows)])
        arrive(("adb",), att.at[t_d, pl.ds(half_rows, half_rows)])
        weight_loads[3].wait()
        width = att.shape[2]
        total = jnp.zeros((rows, cols), jnp.float32)
        for i in range(4):
            total += jnp.dot(
                att[i], wout[i * width : (i + 1) * width, :], preferred_element_type=jnp.float32
            )
        mixer_ref[...] = total.astype(jnp.bfloat16)

    spread(0)
    arrive(("halo", 0), kve.at[pl.ds(0, SIDE)])
    arrive(("halo", 1), kve.at[pl.ds(SIDE + rows, SIDE)])
    rotate_keys()
    attend(0)
    relay(0)
    spread(1)
    attend(1)
    share(0)
    attend(2)
    relay(1)
    attend(3)
    select_back()
    spread(2)
    weight_loads[0].wait()
    weight_loads[1].wait()
    weight_loads[2].wait()
    widen(0, 0)
    share(1)
    widen(0, 1)
    relay(2)
    spread(3)
    attended_out()
    narrow(0)
    share(2)
    widen(1, 0)
    scatter_one(0)
    relay(3)
    widen(1, 1)
    attended_relay()
    narrow(1)
    scatter_two(0)
    share(3)
    widen(2, 0)
    scatter_one(1)
    widen(2, 1)
    narrow(2)
    scatter_two(1)
    widen(3, 0)
    scatter_one(2)
    give_back(1)
    widen(3, 1)
    scatter_two(2)
    narrow(3)
    project()
    scatter_one(3)
    give_back(2)
    give_back(0)
    scatter_two(3)
    give_back(3)
    wait_back(1)
    wait_back(2)
    wait_back(3)
    expert_ref[...] = jnp.dot(
        sel_ret[...], ret[...].reshape(chips * cap, cols), preferred_element_type=jnp.float32
    ).astype(jnp.bfloat16)
    for copy in started:
        copy.wait_send()


def local_fused(
    query_proj, key_proj, value_proj, sink_logit, out_weight, expert_input, norm_gain,
    routes, route_weights, gate_weight, up_weight, down_weight,
):
    rows = query_proj.shape[0]
    tokens, model = expert_input.shape
    cols = out_weight.shape[1]
    hidden = gate_weight.shape[2]
    offset = lax.axis_index("ep") * rows
    cap = tokens // 2
    bf16, f32 = jnp.bfloat16, jnp.float32
    half = HEAD_DIM // 2
    channel = np.arange(2 * HEAD_DIM) % half
    inverse_freq = (1.0 / ROPE_BASE ** (channel * 2.0 / HEAD_DIM)).astype(np.float32)
    far = (offset - SIDE + SIDE * jnp.arange(8, dtype=jnp.int32)).astype(f32)
    far = far[:, None] * inverse_freq[None, :]
    near = np.arange(SIDE)[:, None] * inverse_freq[None, :].astype(np.float64)
    near_tables = [np.cos(near).astype(np.float32), np.sin(near).astype(np.float32)]
    vmem = pl.BlockSpec(memory_space=pltpu.VMEM)
    smem = pl.BlockSpec(memory_space=pltpu.SMEM)
    hbm = pl.BlockSpec(memory_space=pltpu.HBM)
    scratch = [
        pltpu.VMEM(out_weight.shape, bf16),
        pltpu.VMEM((model, hidden), bf16),
        pltpu.VMEM((model, hidden), bf16),
        pltpu.VMEM((hidden, model), bf16),
        pltpu.VMEM((rows + 2 * SIDE, 2 * HEAD_DIM), bf16),
        pltpu.VMEM((rows + 2 * SIDE, 2 * HEAD_DIM), bf16),
        pltpu.VMEM((4, rows, query_proj.shape[1]), bf16),
        pltpu.VMEM((tokens, GROUPS * cap), bf16),
        pltpu.VMEM((GROUPS * cap // 4, model + 128), bf16),
        pltpu.VMEM((GROUPS, 2 * cap, model + 128), bf16),
        pltpu.VMEM((2 * cap, hidden), bf16),
        pltpu.VMEM((GROUPS, 4, 2 * cap, cols), bf16),
        pltpu.VMEM((GROUPS, 4, cap, cols), bf16),
        pltpu.VMEM((GROUPS, 4, cap, cols), bf16),
        pltpu.VMEM((GROUPS, 2, cap // 2, cols), bf16),
        pltpu.VMEM((GROUPS, 2, cap // 2, cols), bf16),
        pltpu.VMEM((GROUPS, 2, cap // 2, cols), bf16),
        pltpu.VMEM((GROUPS, 2, cap // 2, cols), bf16),
        pltpu.VMEM((GROUPS, cap, cols), bf16),
        pltpu.VMEM((GROUPS, cap, cols), bf16),
        pltpu.SemaphoreType.DMA((COPY_SLOTS,)),
        pltpu.SemaphoreType.DMA((COPY_SLOTS,)),
        pltpu.SemaphoreType.DMA((4,)),
    ]
    return pl.pallas_call(
        fused_kernel,
        out_shape=(
            jax.ShapeDtypeStruct((rows, cols), bf16),
            jax.ShapeDtypeStruct((tokens, cols), bf16),
        ),
        in_specs=[vmem] * 7 + [smem] + [vmem] * 4 + [hbm] * 4,
        out_specs=(vmem, vmem),
        scratch_shapes=scratch,
        compiler_params=pltpu.CompilerParams(
            collective_id=0, has_side_effects=True, vmem_limit_bytes=60 * 1024 * 1024
        ),
    )(
        query_proj, key_proj, value_proj, jnp.cos(far), jnp.sin(far), *near_tables,
        sink_logit, expert_input, norm_gain[None, :], routes.T, route_weights.T,
        out_weight, gate_weight[0], up_weight[0], down_weight[0],
    )


def solution(mesh):
    fused = fits_fused(mesh)
    return jax.shard_map(
        local_fused if fused else local,
        mesh=mesh,
        in_specs=(
            P("ep", "tp"),
            P("ep", None),
            P("ep", None),
            P("tp"),
            P(None, "tp"),
            P("ep", None),
            P(),
            P("ep", None),
            P("ep", None),
            P("ep", None, "tp"),
            P("ep", None, "tp"),
            P("ep", "tp", None),
        ),
        out_specs=(P("ep", "tp"), P("ep", "tp")),
        check_vma=False,
    )
```

profile of v0, /device:TPU:0, one launch (start us, length us, event | category | flops | bytes accessed | tf_op | source)
XLA Modules:
  0.0 78.9 jit_solution(10500945986370850606)
XLA Ops:
  0.6 1.4 %multiply_sine_fusion = (f32[8,128]{1,0:T(8,128)}, f32[8,128]{1,0:T(8,128)}) fusion(f32[128]{0:T(128)} %constant.25, f32[8]{0:T(128)S(1)} %add_convert_fusion), kind=kLoop, calls=%fused_computation | loop fusion | flops 1024 | bytes 8736 | tf_op jit(solution)/shard_map/sin | solution.py:634
  2.0 73.3 %shard_map.158 = (bf16[512,512]{1,0:T(8,128)(2,1)}, bf16[256,512]{1,0:T(8,128)(2,1)}) custom-call(bf16[512,256]{1,0:T(8,128)(2,1)} %q_ref.1, bf16[512,256]{1,0:T(8,128)(2,1)} %key_ref.1, bf16[512,256]{1,0:T(8,128)(2,1)} %value_ref.1, f32[8,128]{1,0:T(8,128)} %get-tuple-element.3.cos_far, f32[8,128]{1,0:T(8,128)} %get-tuple-element.2.sin_far, ...), custom_call_target="tpu_custom_call" | custom-call | tf_op jit(solution)/shard_map/pallas_call | solution.py:621
  75.4 1.9 %copy.19 = bf16[512,512]{1,0:T(8,128)(2,1)} copy(bf16[512,512]{1,0:T(8,128)(2,1)} %get-tuple-element.6) | data formatting | bytes 1048576
  77.2 1.7 %copy.20 = bf16[256,512]{1,0:T(8,128)(2,1)} copy(bf16[256,512]{1,0:T(8,128)(2,1)} %get-tuple-element.7) | data formatting | bytes 524288
  (1 shorter events, 0.0 us)
where the time goes:
time: 79.1 us; the launch traced here: 78.9 us
  Pallas kernels  73.3 us (93%)
  local copies, waits for them, and re-layouts  3.54 us (4%)
  other arithmetic  1.37 us (2%)
    pallas_call x1, Pallas kernels, local_fused(): pl.pallas_call(fused_kernel, out_shape=(jax.ShapeDtypeStruct((rows, cols)...  73.3 us
    unnamed x2, local copies, waits for them, and re-layouts  3.54 us

commit v1 on v0

--- a/solution.py
+++ b/solution.py
@@ -210,15 +210,17 @@
         return self.names.setdefault(name, len(self.names))
 
 
-COPY_SLOTS = 96
+RECV_SLOTS = 39
+SEND_SLOTS = 14
 
 
 def fused_kernel(
-    q_ref, key_ref, value_ref, cos_far, sin_far, cos_near, sin_near, sink_ref,
-    x_ref, gain_ref, routes_ref, rw_ref,
-    wout_hbm, wg_hbm, wu_hbm, wd_hbm,
+    x_hbm, routes_hbm, rw_hbm, gain_hbm, key_hbm, value_hbm, q_hbm, table_hbm, sink_hbm,
+    wg_hbm, wu_hbm, wd_hbm, wout_hbm,
     mixer_ref, expert_ref,
-    wout, wg, wu, wd, kve, krot, att, sel_ret, snd, xs, hid, yb, yr, zs, rx, ry, sb, r2, fin, ret,
+    x_ref, routes_ref, rw_ref, gain_ref, key_ref, value_ref, q_ref, table_ref, sink_ref,
+    wg, wu, wd, wout,
+    kve, krot, att, sel_ret, snd, xs, wgt, hid, yb, yr, zs, rx, ry, sb, r2, fin, ret, acc,
     ssem, rsem, wsem,
 ):
     ep = lax.axis_index("ep")
@@ -237,51 +239,44 @@
     half_part, half_cap = part // 2, cap // 2
     hidden = wg.shape[1]
     cols = wout.shape[1]
-    slots = Slots()
-    started = []
-
-    def send(name, src, dst, device):
-        index = slots(*name)
-        copy = pltpu.make_async_remote_copy(
-            src_ref=src, dst_ref=dst, send_sem=ssem.at[index], recv_sem=rsem.at[index],
+    slots, send_slots = Slots(), Slots()
+    z_of = (z, z + 1 - 2 * (z % 2), (z + 2) % chips, chips - 1 - z)
+
+    def remote(send_index, recv_index, src, dst, device):
+        return pltpu.make_async_remote_copy(
+            src_ref=src, dst_ref=dst, send_sem=ssem.at[send_index], recv_sem=rsem.at[recv_index],
             device_id=device, device_id_type=MESH,
         )
-        copy.start()
-        started.append(copy)
+
+    def send(family, name, src, dst, device):
+        remote(send_slots(family), slots(*name), src, dst, device).start()
 
     def arrive(name, dst):
-        index = slots(*name)
-        pltpu.make_async_remote_copy(
-            src_ref=dst, dst_ref=dst, send_sem=ssem.at[index], recv_sem=rsem.at[index],
-            device_id=(ep, t_x), device_id_type=MESH,
-        ).wait_recv()
-
-    def loads():
-        pairs = ((wg_hbm, wg), (wu_hbm, wu), (wd_hbm, wd), (wout_hbm, wout))
-        return [pltpu.make_async_copy(a, b, wsem.at[i]) for i, (a, b) in enumerate(pairs)]
-
-    weight_loads = loads()
-    for copy in weight_loads:
-        copy.start()
+        remote(0, slots(*name), dst, dst, (ep, t_x)).wait_recv()
+
+    def sent(family, src):
+        remote(send_slots(family), 0, src, src, (ep, t_x)).wait_send()
 
     barrier = pltpu.get_barrier_semaphore()
-    peers = [((z + k) % chips * 2 + core, t) for k in range(1, chips)]
+    peers = [(z_of[k] * 2 + core, t) for k in range(1, chips)]
     peers += [(ep, t_x), (ep, t_y), (partner, t), (other, t)]
     for peer in peers:
         pl.semaphore_signal(barrier, inc=1, device_id=peer, device_id_type=MESH)
 
-    row_i = lax.broadcasted_iota(jnp.int32, (key_ref.shape[1], 2 * HEAD_DIM), 0)
-    col_i = lax.broadcasted_iota(jnp.int32, (key_ref.shape[1], 2 * HEAD_DIM), 1)
-    own_key = jnp.where((row_i == t * HEAD_DIM + col_i) & (col_i < HEAD_DIM), 1.0, 0.0)
-    own_value = jnp.where(
-        (row_i == (t - 1) * HEAD_DIM + col_i) & (col_i >= HEAD_DIM), 1.0, 0.0
-    )
-    both = jnp.dot(
-        key_ref[...], own_key.astype(jnp.bfloat16), preferred_element_type=jnp.float32
-    ) + jnp.dot(
-        value_ref[...], own_value.astype(jnp.bfloat16), preferred_element_type=jnp.float32
-    )
-    kve[SIDE : SIDE + rows, :] = both.astype(jnp.bfloat16)
+    pairs = (
+        (x_hbm, x_ref), (routes_hbm, routes_ref), (rw_hbm, rw_ref), (gain_hbm, gain_ref),
+        (key_hbm, key_ref), (value_hbm, value_ref), (q_hbm, q_ref), (table_hbm, table_ref),
+        (sink_hbm, sink_ref), (wg_hbm, wg), (wu_hbm, wu), (wd_hbm, wd), (wout_hbm, wout),
+    )
+    order = (0, 1, 2, 3, 4, 4, 4, 5, 6, 7, 8, 9, 10)
+    loads = [pltpu.make_async_copy(a, b, wsem.at[i]) for i, (a, b) in zip(order, pairs)]
+    for copy in loads[:9]:
+        copy.start()
+    for copy in loads[:4]:
+        copy.wait()
+    for copy in loads[9:]:
+        copy.start()
+
     wide = x_ref[...].astype(jnp.float32)
     inverse = lax.rsqrt(jnp.mean(wide * wide, axis=1, keepdims=True) + NORM_EPS)
     normed = (wide * inverse * gain_ref[...]).astype(jnp.bfloat16)
@@ -293,17 +288,6 @@
     count = jnp.dot(hot.astype(jnp.bfloat16), later, preferred_element_type=jnp.float32)
     rank = jnp.sum(count * hot, axis=0, keepdims=True).astype(jnp.int32)
 
-    slot = lax.broadcasted_iota(jnp.int32, (chips * part, tokens), 0)
-    slot_group = lax.rem(z - slot // part + chips, chips)
-    pick = (group == slot_group) & (rank == t * part + lax.rem(slot, part))
-    pick = jnp.where(pick, 1.0, 0.0).astype(jnp.bfloat16)
-
-    def select_back():
-        slot = lax.broadcasted_iota(jnp.int32, (chips * cap, tokens), 0)
-        slot_group = lax.rem(z - slot // cap + chips, chips)
-        place = (group == slot_group) & (rank == lax.rem(slot, cap))
-        sel_ret[...] = jnp.where(place, 1.0, 0.0).T.astype(jnp.bfloat16)
-
     odd = (routes_ref[...] & 1) == 1
     weight_odd = jnp.sum(jnp.where(odd, rw_ref[...], 0.0), axis=0, keepdims=True)
     weight_even = jnp.sum(jnp.where(odd, 0.0, rw_ref[...]), axis=0, keepdims=True)
@@ -312,50 +296,100 @@
     high = weight.astype(jnp.bfloat16).astype(jnp.float32)
     weight = jnp.where((lane & 1) == 0, high, weight - high)
     weight = jnp.where(lane < 4, weight, 0.0).astype(jnp.bfloat16)
-    snd[:, model:] = lax.dot_general(
-        pick, weight, (((1,), (1,)), ((), ())), preferred_element_type=jnp.float32
-    ).astype(jnp.bfloat16)
-    snd[:, :model] = jnp.dot(pick, normed, preferred_element_type=jnp.float32).astype(jnp.bfloat16)
+
+    def select(pick, out, at):
+        pick = jnp.where(pick, 1.0, 0.0).astype(jnp.bfloat16)
+        out[at, model:] = lax.dot_general(
+            pick, weight, (((1,), (1,)), ((), ())), preferred_element_type=jnp.float32
+        ).astype(jnp.bfloat16)
+        out[at, :model] = jnp.dot(pick, normed, preferred_element_type=jnp.float32).astype(
+            jnp.bfloat16
+        )
+
+    def group_at(index):
+        return jnp.where(
+            index == 0, z_of[0],
+            jnp.where(index == 1, z_of[1], jnp.where(index == 2, z_of[2], z_of[3])),
+        )
+
+    slot = lax.broadcasted_iota(jnp.int32, (chips * part, tokens), 0)
+    index = slot // part
+    owner = jnp.where(index == 1, t_d, t)
+    select(
+        (group == group_at(jnp.maximum(index, 1)))
+        & (rank == owner * part + lax.rem(slot, part)),
+        snd, slice(0, chips * part),
+    )
 
     def piece(k, owner_t, start=0, count=part):
         first = pl.multiple_of(core * cap + owner_t * part + start, 16)
         return xs.at[k, pl.ds(first, count)]
 
-    xs[0, pl.ds(pl.multiple_of(core * cap + t * part, 16), part), :] = snd[0:part, :]
-
-    pl.semaphore_wait(barrier, len(peers))
-    send(("halo", 0), kve.at[pl.ds(rows, SIDE)], kve.at[pl.ds(0, SIDE)], (up, t))
-    send(("halo", 1), kve.at[pl.ds(SIDE, SIDE)], kve.at[pl.ds(SIDE + rows, SIDE)], (down, t))
-    for k in (1, 2, 3):
-        send(
-            ("z", k), snd.at[pl.ds(k * part, part)], piece(k, t),
-            ((z - k + chips) % chips * 2 + core, t),
-        )
-
-    def spread(k):
-        if k:
-            arrive(("z", k), piece(k, t))
-        send(("x", k), piece(k, t), piece(k, t), (ep, t_x))
-        send(("y", k), piece(k, t), piece(k, t), (ep, t_y))
-
-    def relay(k):
-        arrive(("x", k), piece(k, t_x))
-        send(
-            ("da", k), piece(k, t_x, 0, half_part), piece(k, t_x, 0, half_part), (ep, t_y)
-        )
-        arrive(("y", k), piece(k, t_y))
-        send(
-            ("db", k), piece(k, t_y, half_part, half_part),
-            piece(k, t_y, half_part, half_part), (ep, t_x),
-        )
-
     def own_rows(k, which):
         return xs.at[k, pl.ds(pl.multiple_of(which * cap, 16), cap)]
 
+    pltpu.make_async_copy(att.at[pl.ds(0, 3)], att.at[pl.ds(0, 3)], wsem.at[4]).wait()
+    for copy in loads[7:9]:
+        copy.wait()
+    row_i = lax.broadcasted_iota(jnp.int32, (key_ref.shape[1], 2 * HEAD_DIM), 0)
+    col_i = lax.broadcasted_iota(jnp.int32, (key_ref.shape[1], 2 * HEAD_DIM), 1)
+    own_key = jnp.where((row_i == t * HEAD_DIM + col_i) & (col_i < HEAD_DIM), 1.0, 0.0)
+    own_value = jnp.where(
+        (row_i == (t - 1) * HEAD_DIM + col_i) & (col_i >= HEAD_DIM), 1.0, 0.0
+    )
+    both = jnp.dot(
+        key_ref[...], own_key.astype(jnp.bfloat16), preferred_element_type=jnp.float32
+    ) + jnp.dot(
+        value_ref[...], own_value.astype(jnp.bfloat16), preferred_element_type=jnp.float32
+    )
+    kve[SIDE : SIDE + rows, :] = both.astype(jnp.bfloat16)
+
+    pl.semaphore_wait(barrier, len(peers))
+    send("halo", ("halo",), kve.at[pl.ds(rows, SIDE)], kve.at[pl.ds(0, SIDE)], (up, t))
+    send("halo", ("halo",), kve.at[pl.ds(SIDE, SIDE)], kve.at[pl.ds(SIDE + rows, SIDE)], (down, t))
+    for i, (k, owner_t, name) in enumerate(
+        ((1, t, "z"), (1, t_d, "s"), (2, t, "z"), (3, t, "z"))
+    ):
+        send(
+            "z", (name, k), snd.at[pl.ds(i * part, part)], piece(k, owner_t),
+            (z_of[k] * 2 + core, t),
+        )
+
+    slot = lax.broadcasted_iota(jnp.int32, (cap, tokens), 0)
+    select(
+        (group == z) & (rank == slot), xs.at[0], pl.ds(pl.multiple_of(core * cap, 16), cap)
+    )
+    send("p", ("p", 0), own_rows(0, core), own_rows(0, core), (partner, t))
+
+    def select_back():
+        slot = lax.broadcasted_iota(jnp.int32, (chips * cap, tokens), 0)
+        place = (group == group_at(slot // cap)) & (rank == lax.rem(slot, cap))
+        sel_ret[...] = jnp.where(place, 1.0, 0.0).T.astype(jnp.bfloat16)
+
+    def spread(k):
+        arrive(("z", k), piece(k, t))
+        if k == 1:
+            send("x", ("s", k), piece(k, t), piece(k, t), (ep, t_x))
+            send("y", ("s", k), piece(k, t), piece(k, t), (ep, t_y))
+            return
+        for family, name, start, device in (
+            ("x", "xl", 0, t_x), ("y", "yh", half_part, t_y),
+            ("x", "s", half_part, t_x), ("y", "s", 0, t_y),
+        ):
+            rows_of = piece(k, t, start, half_part)
+            send(family, (name, k), rows_of, rows_of, (ep, device))
+
+    def relay(k):
+        arrive(("xl", k), piece(k, t_x, 0, half_part))
+        rows_of = piece(k, t_x, 0, half_part)
+        send("d", ("s", k), rows_of, rows_of, (ep, t_y))
+        arrive(("yh", k), piece(k, t_y, half_part, half_part))
+        rows_of = piece(k, t_y, half_part, half_part)
+        send("d", ("s", k), rows_of, rows_of, (ep, t_x))
+
     def share(k):
-        arrive(("da", k), piece(k, t_d, 0, half_part))
-        arrive(("db", k), piece(k, t_d, half_part, half_part))
-        send(("p", k), own_rows(k, core), own_rows(k, core), (partner, t))
+        arrive(("s", k), snd.at[pl.ds(0, (3 if k == 1 else 2) * part)])
+        send("p", ("p", k), own_rows(k, core), own_rows(k, core), (partner, t))
 
     def swap_matrix(size):
         i = lax.broadcasted_iota(jnp.int32, (size, size), 0)
@@ -366,14 +400,20 @@
         plus = (~low) & (i == j - half)
         return jnp.where(minus, -1.0, jnp.where(plus, 1.0, 0.0)).astype(jnp.bfloat16)
 
+    blocks = rows // SIDE
+    far_rows = (table_ref.shape[0] - 2 * SIDE) // 2
+
     def tables(block):
-        far_c, far_s = cos_far[block : block + 1, :], sin_far[block : block + 1, :]
-        near_c, near_s = cos_near[...], sin_near[...]
+        at = ep * blocks + block
+        far_c = table_ref[pl.ds(at, 1), :]
+        far_s = table_ref[pl.ds(far_rows + at, 1), :]
+        near_c = table_ref[2 * far_rows : 2 * far_rows + SIDE, :]
+        near_s = table_ref[2 * far_rows + SIDE :, :]
         return far_c * near_c - far_s * near_s, far_s * near_c + far_c * near_s
 
-    def rotate_keys():
+    def rotate_keys(which):
         swap = swap_matrix(2 * HEAD_DIM)
-        for block in range(rows // SIDE + 2):
+        for block in which:
             cosine, sine = tables(block)
             raw = kve[block * SIDE : (block + 1) * SIDE, :]
             turned = jnp.dot(raw, swap, preferred_element_type=jnp.float32)
@@ -422,33 +462,43 @@
             [out[h * SIDE : (h + 1) * SIDE, :] for h in range(heads)], axis=1
         )
 
-    def widen(k, half):
-        if half == 0:
-            arrive(("p", k), own_rows(k, 1 - core))
+    def edges():
+        arrive(("halo",), kve.at[pl.ds(0, 2 * SIDE)])
+        rotate_keys((0, blocks + 1))
+
+    tile = 256
+
+    def gather(k):
+        arrive(("p", k), own_rows(k, 1 - core))
         tag = xs[k, :, model:].astype(jnp.float32)
         lane = lax.broadcasted_iota(jnp.int32, tag.shape, 1)
         weight = jnp.sum(jnp.where(lane // 2 == core, tag, 0.0), axis=1, keepdims=True)
-        tile = 256
-        count = hidden // tile // 2
-
-        @pl.loop(half * count, (half + 1) * count)
+        wgt[...] = jnp.broadcast_to(weight, wgt.shape)
+
+    def widen(k, start, stop):
+        @pl.loop(start, stop)
         def _(i):
             at = pl.ds(pl.multiple_of(i * tile, tile), tile)
             gate = jnp.dot(xs[k, :, :model], wg[:, at], preferred_element_type=jnp.float32)
             lift = jnp.dot(xs[k, :, :model], wu[:, at], preferred_element_type=jnp.float32)
             value = gate / (1.0 + jnp.exp(-gate)) * lift
+            weight = jnp.concatenate([wgt[...]] * (tile // wgt.shape[1]), axis=1)
             hid[:, at] = (value * weight).astype(jnp.bfloat16)
 
-    def narrow(k):
-        @pl.loop(0, model // cols)
-        def _(i):
-            at = pl.ds(pl.multiple_of(i * cols, cols), cols)
-            yb[k, i] = jnp.dot(
-                hid[...], wd[:, at], preferred_element_type=jnp.float32
-            ).astype(jnp.bfloat16)
-
+    last = chips - 1
+
+    def target_of(i):
+        return (t_d, t_y, t_x, t)[i]
+
+    def narrow(k, i):
+        target = target_of(i)
+        at = pl.ds(pl.multiple_of(target * cols, cols), cols)
+        yb[k, target] = jnp.dot(hid[...], wd[:, at], preferred_element_type=jnp.float32).astype(
+            jnp.bfloat16
+        )
         theirs = pl.ds(pl.multiple_of((1 - core) * cap, 16), cap)
-        send(("q", k), yb.at[k, :, theirs], yr.at[k], (partner, t))
+        name = ("q", k, i) if k == last else ("q", k)
+        send("q", name, yb.at[k, target, theirs], yr.at[k, target], (partner, t))
 
     def add(*parts):
         return sum(p.astype(jnp.float32) for p in parts).astype(jnp.bfloat16)
@@ -456,54 +506,68 @@
     first, second = slice(0, half_cap), slice(half_cap, cap)
     d_first, d_second = pl.ds(0, half_cap), pl.ds(half_cap, half_cap)
 
-    def scatter_one(k):
-        arrive(("q", k), yr.at[k])
+    def scatter_one(k, i):
+        target = target_of(i)
+        if k == last:
+            arrive(("q", k, i), yr.at[k, target])
+        elif i == 0:
+            arrive(("q", k), yr.at[k])
         mine = pl.ds(pl.multiple_of(core * cap, 16), cap)
-        zs[k] = add(yb[k, :, mine], yr[k])
-        send(("rx", k, 1), zs.at[k, t_d, d_first], rx.at[k, 1], (ep, t_x))
-        send(("ry", k, 1), zs.at[k, t_d, d_second], ry.at[k, 1], (ep, t_y))
-        send(("rx", k, 0), zs.at[k, t_x, d_first], rx.at[k, 0], (ep, t_x))
-        send(("ry", k, 0), zs.at[k, t_y, d_second], ry.at[k, 0], (ep, t_y))
+        zs[k, target] = add(yb[k, target, mine], yr[k, target])
+        if i == 0:
+            send("rx", ("rx", k), zs.at[k, t_d, d_first], rx.at[k, 1], (ep, t_x))
+            send("ry", ("ry", k), zs.at[k, t_d, d_second], ry.at[k, 1], (ep, t_y))
+        if i == 1:
+            send("ry", ("g", k), zs.at[k, t_y, d_second], ry.at[k, 0], (ep, t_y))
+        if i == 2:
+            send("rx", ("g", k), zs.at[k, t_x, d_first], rx.at[k, 0], (ep, t_x))
 
     def scatter_two(k):
-        arrive(("rx", k, 1), rx.at[k, 1])
+        arrive(("rx", k), rx.at[k, 1])
         sb[k, 0] = add(zs[k, t_y, first], rx[k, 1])
-        send(("r2", k, 0), sb.at[k, 0], r2.at[k, 0], (ep, t_y))
-        arrive(("ry", k, 1), ry.at[k, 1])
+        send("r2", ("g", k), sb.at[k, 0], r2.at[k, 0], (ep, t_y))
+        arrive(("ry", k), ry.at[k, 1])
         sb[k, 1] = add(zs[k, t_x, second], ry[k, 1])
-        send(("r2", k, 1), sb.at[k, 1], r2.at[k, 1], (ep, t_x))
+        send("r2", ("g", k), sb.at[k, 1], r2.at[k, 1], (ep, t_x))
 
     def give_back(k):
-        arrive(("rx", k, 0), rx.at[k, 0])
-        arrive(("ry", k, 0), ry.at[k, 0])
-        arrive(("r2", k, 0), r2.at[k, 0])
-        arrive(("r2", k, 1), r2.at[k, 1])
+        arrive(("g", k), r2.at[pl.ds(0, 2)])
         target = fin if k else ret
         target[k, first] = add(zs[k, t, first], rx[k, 0], r2[k, 0])
         target[k, second] = add(zs[k, t, second], ry[k, 0], r2[k, 1])
         if k:
-            send(("ret", k), fin.at[k], ret.at[k], ((z + k) % chips * 2 + core, t))
-
-    def wait_back(k):
-        arrive(("ret", k), ret.at[k])
-
-    half_rows = rows // 2
-
-    def attended_out():
-        send(("ax",), att.at[t], att.at[t], (ep, t_x))
-        send(("ay",), att.at[t], att.at[t], (ep, t_y))
-
-    def attended_relay():
-        low, high = pl.ds(0, half_rows), pl.ds(half_rows, half_rows)
-        arrive(("ax",), att.at[t_x])
-        send(("ada",), att.at[t_x, low], att.at[t_x, low], (ep, t_y))
-        arrive(("ay",), att.at[t_y])
-        send(("adb",), att.at[t_y, high], att.at[t_y, high], (ep, t_x))
+            name = ("ret", last) if k == last else ("ret",)
+            send("ret", name, fin.at[k], ret.at[k], (z_of[k] * 2 + core, t))
+
+    def wait_back_early():
+        arrive(("ret",), ret.at[pl.ds(1, last - 1)])
+
+    def wait_back():
+        arrive(("ret", last), ret.at[last])
+
+    mid = pl.ds(SIDE, rows - 2 * SIDE)
+    ends = (pl.ds(0, SIDE), pl.ds(rows - SIDE, SIDE))
+
+    def attended_mid():
+        send("ax", ("axm",), att.at[t, mid], att.at[t, mid], (ep, t_x))
+        send("ay", ("proj",), att.at[t, mid], att.at[t, mid], (ep, t_y))
+
+    def attended_ends():
+        for at in ends:
+            send("ay", ("aye",), att.at[t, at], att.at[t, at], (ep, t_y))
+            send("ax", ("proj",), att.at[t, at], att.at[t, at], (ep, t_x))
+
+    def attended_relay_mid():
+        arrive(("axm",), att.at[t_x, mid])
+        send("ad", ("proj",), att.at[t_x, mid], att.at[t_x, mid], (ep, t_y))
+
+    def attended_relay_ends():
+        arrive(("aye",), att.at[t_y, pl.ds(0, 2 * SIDE)])
+        for at in ends:
+            send("ad", ("proj",), att.at[t_y, at], att.at[t_y, at], (ep, t_x))
 
     def project():
-        arrive(("ada",), att.at[t_d, pl.ds(0, half_rows)])
-        arrive(("adb",), att.at[t_d, pl.ds(half_rows, half_rows)])
-        weight_loads[3].wait()
+        arrive(("proj",), att.at[pl.ds(0, 2)])
         width = att.shape[2]
         total = jnp.zeros((rows, cols), jnp.float32)
         for i in range(4):
@@ -512,64 +576,113 @@
             )
         mixer_ref[...] = total.astype(jnp.bfloat16)
 
-    spread(0)
-    arrive(("halo", 0), kve.at[pl.ds(0, SIDE)])
-    arrive(("halo", 1), kve.at[pl.ds(SIDE + rows, SIDE)])
-    rotate_keys()
+    def load_wait(i):
+        loads[9 + i].wait()
+
+    def place_early():
+        count = (chips - 1) * cap
+        acc[...] = jnp.dot(
+            sel_ret[:, :count], ret[: chips - 1].reshape(count, cols),
+            preferred_element_type=jnp.float32,
+        )
+
+    def place_last():
+        count = (chips - 1) * cap
+        expert_ref[...] = (
+            acc[...]
+            + jnp.dot(sel_ret[:, count:], ret[chips - 1], preferred_element_type=jnp.float32)
+        ).astype(jnp.bfloat16)
+
+    rotate_keys(range(1, blocks + 1))
+    attend(1)
+    attend(2)
+    attended_mid()
+    edges()
     attend(0)
-    relay(0)
+    load_wait(0)
+    load_wait(1)
+    gather(0)
+    widen(0, 0, 1)
     spread(1)
-    attend(1)
-    share(0)
-    attend(2)
-    relay(1)
+    widen(0, 1, 3)
+    attended_relay_mid()
     attend(3)
+    attended_ends()
+    widen(0, 3, 4)
+    share(1)
+    load_wait(2)
+    narrow(0, 0)
+    narrow(0, 1)
+    narrow(0, 2)
+    narrow(0, 3)
     select_back()
     spread(2)
-    weight_loads[0].wait()
-    weight_loads[1].wait()
-    weight_loads[2].wait()
-    widen(0, 0)
-    share(1)
-    widen(0, 1)
+    gather(1)
+    widen(1, 0, 1)
+    scatter_one(0, 0)
+    scatter_one(0, 1)
+    scatter_one(0, 2)
+    scatter_one(0, 3)
+    widen(1, 1, 2)
     relay(2)
     spread(3)
-    attended_out()
-    narrow(0)
+    widen(1, 2, 4)
+    attended_relay_ends()
+    scatter_two(0)
+    narrow(1, 0)
+    narrow(1, 1)
+    narrow(1, 2)
+    narrow(1, 3)
     share(2)
-    widen(1, 0)
-    scatter_one(0)
     relay(3)
-    widen(1, 1)
-    attended_relay()
-    narrow(1)
-    scatter_two(0)
+    scatter_one(1, 0)
+    scatter_one(1, 1)
+    scatter_one(1, 2)
+    scatter_one(1, 3)
+    gather(2)
+    widen(2, 0, 2)
     share(3)
-    widen(2, 0)
-    scatter_one(1)
-    widen(2, 1)
-    narrow(2)
+    give_back(0)
+    widen(2, 2, 4)
     scatter_two(1)
-    widen(3, 0)
-    scatter_one(2)
+    narrow(2, 0)
+    narrow(2, 1)
+    narrow(2, 2)
+    narrow(2, 3)
+    gather(3)
+    widen(3, 0, 1)
+    scatter_one(2, 0)
+    scatter_one(2, 1)
+    scatter_one(2, 2)
+    scatter_one(2, 3)
     give_back(1)
-    widen(3, 1)
+    widen(3, 1, 4)
     scatter_two(2)
-    narrow(3)
+    narrow(3, 0)
+    narrow(3, 1)
+    narrow(3, 2)
+    scatter_one(3, 0)
+    narrow(3, 3)
+    scatter_one(3, 1)
+    scatter_one(3, 2)
+    scatter_one(3, 3)
+    give_back(2)
+    load_wait(3)
     project()
-    scatter_one(3)
-    give_back(2)
-    give_back(0)
     scatter_two(3)
+    wait_back_early()
+    place_early()
     give_back(3)
-    wait_back(1)
-    wait_back(2)
-    wait_back(3)
-    expert_ref[...] = jnp.dot(
-        sel_ret[...], ret[...].reshape(chips * cap, cols), preferred_element_type=jnp.float32
-    ).astype(jnp.bfloat16)
-    for copy in started:
-        copy.wait_send()
+    wait_back()
+    place_last()
+    for family, ref in (
+        ("halo", kve.at[pl.ds(0, 2 * SIDE)]), ("z", snd), ("p", xs.at[:, pl.ds(0, cap)]),
+        ("x", snd.at[pl.ds(0, 3 * part)]), ("y", snd.at[pl.ds(0, 3 * part)]),
+        ("d", snd.at[pl.ds(0, 2 * part)]), ("q", yr), ("rx", rx), ("ry", ry), ("r2", r2),
+        ("ret", fin.at[pl.ds(1, last)]), ("ax", att.at[0]), ("ay", att.at[0]),
+        ("ad", att.at[0]),
+    ):
+        sent(family, ref)
 
 
 def local_fused(
@@ -580,30 +693,34 @@
     tokens, model = expert_input.shape
     cols = out_weight.shape[1]
     hidden = gate_weight.shape[2]
-    offset = lax.axis_index("ep") * rows
     cap = tokens // 2
     bf16, f32 = jnp.bfloat16, jnp.float32
     half = HEAD_DIM // 2
     channel = np.arange(2 * HEAD_DIM) % half
-    inverse_freq = (1.0 / ROPE_BASE ** (channel * 2.0 / HEAD_DIM)).astype(np.float32)
-    far = (offset - SIDE + SIDE * jnp.arange(8, dtype=jnp.int32)).astype(f32)
-    far = far[:, None] * inverse_freq[None, :]
-    near = np.arange(SIDE)[:, None] * inverse_freq[None, :].astype(np.float64)
-    near_tables = [np.cos(near).astype(np.float32), np.sin(near).astype(np.float32)]
+    inverse_freq = 1.0 / ROPE_BASE ** (channel * 2.0 / HEAD_DIM)
+    far_count = -(-(lax.axis_size("ep") * (rows // SIDE) + 2) // 8) * 8
+    far = (np.arange(far_count) - 1)[:, None] * SIDE * inverse_freq[None, :]
+    near = np.arange(SIDE)[:, None] * inverse_freq[None, :]
+    table = np.concatenate([np.cos(far), np.sin(far), np.cos(near), np.sin(near)]).astype(
+        np.float32
+    )
+    hbm = pl.BlockSpec(memory_space=pltpu.HBM)
     vmem = pl.BlockSpec(memory_space=pltpu.VMEM)
-    smem = pl.BlockSpec(memory_space=pltpu.SMEM)
-    hbm = pl.BlockSpec(memory_space=pltpu.HBM)
+    args = (
+        expert_input, routes.T, route_weights.T, norm_gain[None, :], key_proj, value_proj,
+        query_proj, jnp.asarray(table), sink_logit, gate_weight[0], up_weight[0], down_weight[0],
+        out_weight,
+    )
     scratch = [
-        pltpu.VMEM(out_weight.shape, bf16),
-        pltpu.VMEM((model, hidden), bf16),
-        pltpu.VMEM((model, hidden), bf16),
-        pltpu.VMEM((hidden, model), bf16),
+        (pltpu.SMEM if a is sink_logit else pltpu.VMEM)(a.shape, a.dtype) for a in args
+    ] + [
         pltpu.VMEM((rows + 2 * SIDE, 2 * HEAD_DIM), bf16),
         pltpu.VMEM((rows + 2 * SIDE, 2 * HEAD_DIM), bf16),
         pltpu.VMEM((4, rows, query_proj.shape[1]), bf16),
         pltpu.VMEM((tokens, GROUPS * cap), bf16),
-        pltpu.VMEM((GROUPS * cap // 4, model + 128), bf16),
+        pltpu.VMEM((cap, model + 128), bf16),
         pltpu.VMEM((GROUPS, 2 * cap, model + 128), bf16),
+        pltpu.VMEM((2 * cap, 128), f32),
         pltpu.VMEM((2 * cap, hidden), bf16),
         pltpu.VMEM((GROUPS, 4, 2 * cap, cols), bf16),
         pltpu.VMEM((GROUPS, 4, cap, cols), bf16),
@@ -614,27 +731,21 @@
         pltpu.VMEM((GROUPS, 2, cap // 2, cols), bf16),
         pltpu.VMEM((GROUPS, cap, cols), bf16),
         pltpu.VMEM((GROUPS, cap, cols), bf16),
-        pltpu.SemaphoreType.DMA((COPY_SLOTS,)),
-        pltpu.SemaphoreType.DMA((COPY_SLOTS,)),
-        pltpu.SemaphoreType.DMA((4,)),
+        pltpu.VMEM((tokens, cols), f32),
+        pltpu.SemaphoreType.DMA((SEND_SLOTS,)),
+        pltpu.SemaphoreType.DMA((RECV_SLOTS,)),
+        pltpu.SemaphoreType.DMA((len(args) - 2,)),
     ]
     return pl.pallas_call(
         fused_kernel,
-        out_shape=(
-            jax.ShapeDtypeStruct((rows, cols), bf16),
-            jax.ShapeDtypeStruct((tokens, cols), bf16),
-        ),
-        in_specs=[vmem] * 7 + [smem] + [vmem] * 4 + [hbm] * 4,
+        out_shape=(pltpu.VMEM((rows, cols), bf16), pltpu.VMEM((tokens, cols), bf16)),
+        in_specs=[hbm] * len(args),
         out_specs=(vmem, vmem),
         scratch_shapes=scratch,
         compiler_params=pltpu.CompilerParams(
             collective_id=0, has_side_effects=True, vmem_limit_bytes=60 * 1024 * 1024
         ),
-    )(
-        query_proj, key_proj, value_proj, jnp.cos(far), jnp.sin(far), *near_tables,
-        sink_logit, expert_input, norm_gain[None, :], routes.T, route_weights.T,
-        out_weight, gate_weight[0], up_weight[0], down_weight[0],
-    )
+    )(*args)
 
 
 def solution(mesh):

time: 79.1 us -> 64.1 us (0.81)
  Pallas kernels: 73.3 us -> 61.8 us
  local copies, waits for them, and re-layouts: 3.54 us -> 1.5 us
  other arithmetic: 1.37 us -> 0 us
    pallas_call x1, Pallas kernels: 73.3 us -> 61.8 us  [local_fused(): pl.pallas_call(fused_kernel, out_shape=(pltpu.VMEM((rows, cols), bf16), p...]
    unnamed x2, local copies, waits for them, and re-layouts: 3.54 us -> 1.5 us
    sin x1 -> x0, other arithmetic: 1.37 us -> none  [local_fused(): jnp.sin(far)]
where the time goes in v1:
time: 64.1 us; the launch traced here: 64 us
  Pallas kernels  61.8 us (96%)
  local copies, waits for them, and re-layouts  1.5 us (2%)
    pallas_call x1, Pallas kernels, local_fused(): pl.pallas_call(fused_kernel, out_shape=(pltpu.VMEM((rows, cols), bf16), p...  61.8 us
    unnamed x2, local copies, waits for them, and re-layouts  1.5 us

profile of v1, /device:TPU:0, one launch (start us, length us, event | category | flops | bytes accessed | tf_op | source)
XLA Modules:
  0.0 64.0 jit_solution(12750991744202045008)
XLA Ops:
  0.6 61.8 %shard_map.140 = (bf16[512,512]{1,0:T(8,128)(2,1)S(1)}, bf16[256,512]{1,0:T(8,128)(2,1)S(1)}) custom-call(bf16[256,2048]{1,0:T(8,128)(2,1)} %x_hbm.1, s32[2,256]{1,0:T(2,128)} %bitcast.10, f32[2,256]{1,0:T(2,128)} %bitcast.11, f32[1,2048]{1,0:T(1,128)} %bitcast.9, bf16[512,256]{1,0:T(8,128)(2,1)} %key_hbm.1, bf16[512,256]{1,0:T(8,128)(2,1)} %value_hbm.1, ...), custom_call_target="tpu_custom_call" | custom-call | tf_op jit(solution)/shard_map/pallas_call | solution.py:739
  62.5 0.8 %copy.17 = bf16[512,512]{1,0:T(8,128)(2,1)} copy(bf16[512,512]{1,0:T(8,128)(2,1)S(1)} %get-tuple-element.2) | data formatting | bytes 1048576
  63.3 0.7 %copy.18 = bf16[256,512]{1,0:T(8,128)(2,1)} copy(bf16[256,512]{1,0:T(8,128)(2,1)S(1)} %get-tuple-element.3) | data formatting | bytes 524288

commit v2 on v1

--- a/solution.py
+++ b/solution.py
@@ -210,7 +210,7 @@
         return self.names.setdefault(name, len(self.names))
 
 
-RECV_SLOTS = 39
+RECV_SLOTS = 40
 SEND_SLOTS = 14
 
 
@@ -312,13 +312,14 @@
             jnp.where(index == 1, z_of[1], jnp.where(index == 2, z_of[2], z_of[3])),
         )
 
-    slot = lax.broadcasted_iota(jnp.int32, (chips * part, tokens), 0)
+    pieces = ((1, t, "z"), (2, t, "z"), (1, t_d, "s"), (3, t, "z"), (3, t_d, "s"))
+    slot = lax.broadcasted_iota(jnp.int32, (len(pieces) * part, tokens), 0)
     index = slot // part
-    owner = jnp.where(index == 1, t_d, t)
+    owner = jnp.where((index == 2) | (index == 4), t_d, t)
+    step = jnp.where(index == 1, 2, jnp.where(index >= 3, 3, 1))
     select(
-        (group == group_at(jnp.maximum(index, 1)))
-        & (rank == owner * part + lax.rem(slot, part)),
-        snd, slice(0, chips * part),
+        (group == group_at(step)) & (rank == owner * part + lax.rem(slot, part)), snd,
+        slice(0, len(pieces) * part),
     )
 
     def piece(k, owner_t, start=0, count=part):
@@ -347,13 +348,14 @@
     pl.semaphore_wait(barrier, len(peers))
     send("halo", ("halo",), kve.at[pl.ds(rows, SIDE)], kve.at[pl.ds(0, SIDE)], (up, t))
     send("halo", ("halo",), kve.at[pl.ds(SIDE, SIDE)], kve.at[pl.ds(SIDE + rows, SIDE)], (down, t))
-    for i, (k, owner_t, name) in enumerate(
-        ((1, t, "z"), (1, t_d, "s"), (2, t, "z"), (3, t, "z"))
-    ):
+    def dispatch(i):
+        k, owner_t, name = pieces[i]
         send(
             "z", (name, k), snd.at[pl.ds(i * part, part)], piece(k, owner_t),
             (z_of[k] * 2 + core, t),
         )
+
+    dispatch(0)
 
     slot = lax.broadcasted_iota(jnp.int32, (cap, tokens), 0)
     select(
@@ -368,7 +370,7 @@
 
     def spread(k):
         arrive(("z", k), piece(k, t))
-        if k == 1:
+        if k != 2:
             send("x", ("s", k), piece(k, t), piece(k, t), (ep, t_x))
             send("y", ("s", k), piece(k, t), piece(k, t), (ep, t_y))
             return
@@ -379,16 +381,14 @@
             rows_of = piece(k, t, start, half_part)
             send(family, (name, k), rows_of, rows_of, (ep, device))
 
-    def relay(k):
-        arrive(("xl", k), piece(k, t_x, 0, half_part))
-        rows_of = piece(k, t_x, 0, half_part)
-        send("d", ("s", k), rows_of, rows_of, (ep, t_y))
-        arrive(("yh", k), piece(k, t_y, half_part, half_part))
-        rows_of = piece(k, t_y, half_part, half_part)
-        send("d", ("s", k), rows_of, rows_of, (ep, t_x))
+    def relay(k, half):
+        name, source, target = (("xl", t_x, t_y), ("yh", t_y, t_x))[half]
+        rows_of = piece(k, source, half * half_part, half_part)
+        arrive((name, k), rows_of)
+        send("d", ("s", k), rows_of, rows_of, (ep, target))
 
     def share(k):
-        arrive(("s", k), snd.at[pl.ds(0, (3 if k == 1 else 2) * part)])
+        arrive(("s", k), snd.at[pl.ds(0, (2 if k == 2 else 3) * part)])
         send("p", ("p", k), own_rows(k, core), own_rows(k, core), (partner, t))
 
     def swap_matrix(size):
@@ -476,9 +476,8 @@
         wgt[...] = jnp.broadcast_to(weight, wgt.shape)
 
     def widen(k, start, stop):
-        @pl.loop(start, stop)
-        def _(i):
-            at = pl.ds(pl.multiple_of(i * tile, tile), tile)
+        for i in range(start, stop):
+            at = pl.ds(i * tile, tile)
             gate = jnp.dot(xs[k, :, :model], wg[:, at], preferred_element_type=jnp.float32)
             lift = jnp.dot(xs[k, :, :model], wu[:, at], preferred_element_type=jnp.float32)
             value = gate / (1.0 + jnp.exp(-gate)) * lift
@@ -497,7 +496,7 @@
             jnp.bfloat16
         )
         theirs = pl.ds(pl.multiple_of((1 - core) * cap, 16), cap)
-        name = ("q", k, i) if k == last else ("q", k)
+        name = ("q", k, i) if k >= 2 else ("q", k)
         send("q", name, yb.at[k, target, theirs], yr.at[k, target], (partner, t))
 
     def add(*parts):
@@ -506,14 +505,16 @@
     first, second = slice(0, half_cap), slice(half_cap, cap)
     d_first, d_second = pl.ds(0, half_cap), pl.ds(half_cap, half_cap)
 
-    def scatter_one(k, i):
+    def scatter_add(k, i):
         target = target_of(i)
-        if k == last:
+        if k >= 2:
             arrive(("q", k, i), yr.at[k, target])
         elif i == 0:
             arrive(("q", k), yr.at[k])
         mine = pl.ds(pl.multiple_of(core * cap, 16), cap)
         zs[k, target] = add(yb[k, target, mine], yr[k, target])
+
+    def scatter_send(k, i):
         if i == 0:
             send("rx", ("rx", k), zs.at[k, t_d, d_first], rx.at[k, 1], (ep, t_x))
             send("ry", ("ry", k), zs.at[k, t_d, d_second], ry.at[k, 1], (ep, t_y))
@@ -521,6 +522,10 @@
             send("ry", ("g", k), zs.at[k, t_y, d_second], ry.at[k, 0], (ep, t_y))
         if i == 2:
             send("rx", ("g", k), zs.at[k, t_x, d_first], rx.at[k, 0], (ep, t_x))
+
+    def scatter_one(k, i):
+        scatter_add(k, i)
+        scatter_send(k, i)
 
     def scatter_two(k):
         arrive(("rx", k), rx.at[k, 1])
@@ -595,90 +600,95 @@
 
     rotate_keys(range(1, blocks + 1))
     attend(1)
+    dispatch(1)
+    dispatch(2)
     attend(2)
     attended_mid()
+    dispatch(3)
     edges()
     attend(0)
+    attend(3)
+    attended_ends()
     load_wait(0)
     load_wait(1)
     gather(0)
-    widen(0, 0, 1)
+    widen(0, 0, 2)
     spread(1)
-    widen(0, 1, 3)
-    attended_relay_mid()
-    attend(3)
-    attended_ends()
-    widen(0, 3, 4)
-    share(1)
+    widen(0, 2, 4)
     load_wait(2)
     narrow(0, 0)
     narrow(0, 1)
     narrow(0, 2)
     narrow(0, 3)
+    spread(2)
+    dispatch(4)
     select_back()
-    spread(2)
+    share(1)
+    relay(2, 0)
+    scatter_add(0, 0)
+    scatter_add(0, 1)
+    scatter_add(0, 2)
+    scatter_add(0, 3)
     gather(1)
-    widen(1, 0, 1)
-    scatter_one(0, 0)
-    scatter_one(0, 1)
-    scatter_one(0, 2)
-    scatter_one(0, 3)
-    widen(1, 1, 2)
-    relay(2)
+    relay(2, 1)
+    widen(1, 0, 2)
+    attended_relay_mid()
+    attended_relay_ends()
+    widen(1, 2, 4)
+    narrow(1, 0)
     spread(3)
-    widen(1, 2, 4)
-    attended_relay_ends()
-    scatter_two(0)
-    narrow(1, 0)
     narrow(1, 1)
     narrow(1, 2)
+    share(2)
     narrow(1, 3)
-    share(2)
-    relay(3)
+    scatter_send(0, 0)
+    scatter_send(0, 1)
+    scatter_send(0, 2)
+    gather(2)
+    widen(2, 0, 1)
     scatter_one(1, 0)
     scatter_one(1, 1)
     scatter_one(1, 2)
     scatter_one(1, 3)
-    gather(2)
-    widen(2, 0, 2)
-    share(3)
-    give_back(0)
-    widen(2, 2, 4)
-    scatter_two(1)
+    widen(2, 1, 4)
     narrow(2, 0)
     narrow(2, 1)
+    share(3)
+    scatter_one(2, 0)
     narrow(2, 2)
+    scatter_one(2, 1)
     narrow(2, 3)
+    scatter_one(2, 2)
     gather(3)
     widen(3, 0, 1)
-    scatter_one(2, 0)
-    scatter_one(2, 1)
-    scatter_one(2, 2)
     scatter_one(2, 3)
-    give_back(1)
+    scatter_two(1)
     widen(3, 1, 4)
-    scatter_two(2)
     narrow(3, 0)
     narrow(3, 1)
+    scatter_two(2)
     narrow(3, 2)
     scatter_one(3, 0)
     narrow(3, 3)
     scatter_one(3, 1)
     scatter_one(3, 2)
     scatter_one(3, 3)
-    give_back(2)
+    give_back(1)
     load_wait(3)
     project()
+    give_back(2)
     scatter_two(3)
+    scatter_two(0)
+    give_back(3)
+    give_back(0)
     wait_back_early()
     place_early()
-    give_back(3)
     wait_back()
     place_last()
     for family, ref in (
         ("halo", kve.at[pl.ds(0, 2 * SIDE)]), ("z", snd), ("p", xs.at[:, pl.ds(0, cap)]),
         ("x", snd.at[pl.ds(0, 3 * part)]), ("y", snd.at[pl.ds(0, 3 * part)]),
-        ("d", snd.at[pl.ds(0, 2 * part)]), ("q", yr), ("rx", rx), ("ry", ry), ("r2", r2),
+        ("d", snd.at[pl.ds(0, part)]), ("q", yr), ("rx", rx), ("ry", ry), ("r2", r2),
         ("ret", fin.at[pl.ds(1, last)]), ("ax", att.at[0]), ("ay", att.at[0]),
         ("ad", att.at[0]),
     ):
@@ -718,7 +728,7 @@
         pltpu.VMEM((rows + 2 * SIDE, 2 * HEAD_DIM), bf16),
         pltpu.VMEM((4, rows, query_proj.shape[1]), bf16),
         pltpu.VMEM((tokens, GROUPS * cap), bf16),
-        pltpu.VMEM((cap, model + 128), bf16),
+        pltpu.VMEM((5 * cap // 4, model + 128), bf16),
         pltpu.VMEM((GROUPS, 2 * cap, model + 128), bf16),
         pltpu.VMEM((2 * cap, 128), f32),
         pltpu.VMEM((2 * cap, hidden), bf16),

time: 64.1 us -> 55.4 us (0.86)
  Pallas kernels: 61.8 us -> 52.7 us
    pallas_call x1, Pallas kernels: 61.8 us -> 52.7 us  [local_fused(): pl.pallas_call(fused_kernel, out_shape=(pltpu.VMEM((rows, cols), bf16), p...]
where the time goes in v2:
time: 55.4 us; the launch traced here: 54.8 us
  Pallas kernels  52.7 us (95%)
  local copies, waits for them, and re-layouts  1.5 us (3%)
  between operations  0.64 us (1%)
    pallas_call x1, Pallas kernels, local_fused(): pl.pallas_call(fused_kernel, out_shape=(pltpu.VMEM((rows, cols), bf16), p...  52.7 us
    unnamed x2, local copies, waits for them, and re-layouts  1.5 us

profile of v2, /device:TPU:0, one launch (start us, length us, event | category | flops | bytes accessed | tf_op | source)
XLA Modules:
  0.0 54.8 jit_solution(4136420700021731692)
XLA Ops:
  0.6 52.7 %shard_map.140 = (bf16[512,512]{1,0:T(8,128)(2,1)S(1)}, bf16[256,512]{1,0:T(8,128)(2,1)S(1)}) custom-call(bf16[256,2048]{1,0:T(8,128)(2,1)} %x_hbm.1, s32[2,256]{1,0:T(2,128)} %bitcast.10, f32[2,256]{1,0:T(2,128)} %bitcast.11, f32[1,2048]{1,0:T(1,128)} %bitcast.9, bf16[512,256]{1,0:T(8,128)(2,1)} %key_hbm.1, bf16[512,256]{1,0:T(8,128)(2,1)} %value_hbm.1, ...), custom_call_target="tpu_custom_call" | custom-call | tf_op jit(solution)/shard_map/pallas_call | solution.py:749
  53.3 0.8 %copy.17 = bf16[512,512]{1,0:T(8,128)(2,1)} copy(bf16[512,512]{1,0:T(8,128)(2,1)S(1)} %get-tuple-element.2) | data formatting | bytes 1048576
  54.1 0.7 %copy.18 = bf16[256,512]{1,0:T(8,128)(2,1)} copy(bf16[256,512]{1,0:T(8,128)(2,1)S(1)} %get-tuple-element.3) | data formatting | bytes 524288

commit v3 on v2

--- a/solution.py
+++ b/solution.py
@@ -489,15 +489,18 @@
     def target_of(i):
         return (t_d, t_y, t_x, t)[i]
 
-    def narrow(k, i):
-        target = target_of(i)
-        at = pl.ds(pl.multiple_of(target * cols, cols), cols)
-        yb[k, target] = jnp.dot(hid[...], wd[:, at], preferred_element_type=jnp.float32).astype(
-            jnp.bfloat16
-        )
+    def narrow(k, *chunks):
         theirs = pl.ds(pl.multiple_of((1 - core) * cap, 16), cap)
-        name = ("q", k, i) if k >= 2 else ("q", k)
-        send("q", name, yb.at[k, target, theirs], yr.at[k, target], (partner, t))
+        for i in chunks:
+            target = target_of(i)
+            at = pl.ds(pl.multiple_of(target * cols, cols), cols)
+            yb[k, target] = jnp.dot(
+                hid[...], wd[:, at], preferred_element_type=jnp.float32
+            ).astype(jnp.bfloat16)
+        for i in chunks:
+            target = target_of(i)
+            name = ("q", k, i) if k >= 2 else ("q", k)
+            send("q", name, yb.at[k, target, theirs], yr.at[k, target], (partner, t))
 
     def add(*parts):
         return sum(p.astype(jnp.float32) for p in parts).astype(jnp.bfloat16)
@@ -616,10 +619,7 @@
     spread(1)
     widen(0, 2, 4)
     load_wait(2)
-    narrow(0, 0)
-    narrow(0, 1)
-    narrow(0, 2)
-    narrow(0, 3)
+    narrow(0, 0, 1, 2, 3)
     spread(2)
     dispatch(4)
     select_back()
@@ -637,13 +637,9 @@
     widen(1, 2, 4)
     narrow(1, 0)
     spread(3)
-    narrow(1, 1)
-    narrow(1, 2)
+    narrow(1, 1, 2)
     share(2)
     narrow(1, 3)
-    scatter_send(0, 0)
-    scatter_send(0, 1)
-    scatter_send(0, 2)
     gather(2)
     widen(2, 0, 1)
     scatter_one(1, 0)
@@ -651,8 +647,7 @@
     scatter_one(1, 2)
     scatter_one(1, 3)
     widen(2, 1, 4)
-    narrow(2, 0)
-    narrow(2, 1)
+    narrow(2, 0, 1)
     share(3)
     scatter_one(2, 0)
     narrow(2, 2)
@@ -664,8 +659,7 @@
     scatter_one(2, 3)
     scatter_two(1)
     widen(3, 1, 4)
-    narrow(3, 0)
-    narrow(3, 1)
+    narrow(3, 0, 1)
     scatter_two(2)
     narrow(3, 2)
     scatter_one(3, 0)
@@ -678,8 +672,11 @@
     project()
     give_back(2)
     scatter_two(3)
+    scatter_send(0, 0)
+    scatter_send(0, 1)
+    scatter_send(0, 2)
+    give_back(3)
     scatter_two(0)
-    give_back(3)
     give_back(0)
     wait_back_early()
     place_early()

time: 55.4 us -> 54.6 us (0.986)
  Pallas kernels: 52.7 us -> 51.9 us
    pallas_call x1, Pallas kernels: 52.7 us -> 51.9 us  [local_fused(): pl.pallas_call(fused_kernel, out_shape=(pltpu.VMEM((rows, cols), bf16), p...]
where the time goes in v3:
time: 54.6 us; the launch traced here: 54 us
  Pallas kernels  51.9 us (95%)
  local copies, waits for them, and re-layouts  1.5 us (3%)
  between operations  0.64 us (1%)
    pallas_call x1, Pallas kernels, local_fused(): pl.pallas_call(fused_kernel, out_shape=(pltpu.VMEM((rows, cols), bf16), p...  51.9 us
    unnamed x2, local copies, waits for them, and re-layouts  1.5 us

profile of v3, /device:TPU:0, one launch (start us, length us, event | category | flops | bytes accessed | tf_op | source)
XLA Modules:
  0.0 54.0 jit_solution(13405922283113270510)
XLA Ops:
  0.6 51.9 %shard_map.140 = (bf16[512,512]{1,0:T(8,128)(2,1)S(1)}, bf16[256,512]{1,0:T(8,128)(2,1)S(1)}) custom-call(bf16[256,2048]{1,0:T(8,128)(2,1)} %x_hbm.1, s32[2,256]{1,0:T(2,128)} %bitcast.10, f32[2,256]{1,0:T(2,128)} %bitcast.11, f32[1,2048]{1,0:T(1,128)} %bitcast.9, bf16[512,256]{1,0:T(8,128)(2,1)} %key_hbm.1, bf16[512,256]{1,0:T(8,128)(2,1)} %value_hbm.1, ...), custom_call_target="tpu_custom_call" | custom-call | tf_op jit(solution)/shard_map/pallas_call | solution.py:746
  52.5 0.8 %copy.17 = bf16[512,512]{1,0:T(8,128)(2,1)} copy(bf16[512,512]{1,0:T(8,128)(2,1)S(1)} %get-tuple-element.2) | data formatting | bytes 1048576
  53.3 0.7 %copy.18 = bf16[256,512]{1,0:T(8,128)(2,1)} copy(bf16[256,512]{1,0:T(8,128)(2,1)S(1)} %get-tuple-element.3) | data formatting | bytes 524288
